TPU v7x, 512 devices: a 8x2x16 block of a 8x16x16 slice. The times are simulated.
512 devices in a mesh: grp: 2 (over y), sp: 16 (over z), tp: 16 (over x, core).
Axes of the slice: x: 8, y: 2, z: 16, core: 2. Of those that a mesh axis runs over, the one named last changes fastest.
The devices are a block of a 8x16x16 slice.
Arguments:
- tokens: bfloat16 [8192, 2048], P(('grp', 'sp'), 'tp'), parts along dimension 0, may hold values from -40 to 40
- norm_gain: float32 [2, 2048], replicated, may hold values from 0.1 to 1.9
- value_proj: bfloat16 [2, 1024, 2048], P(None, 'tp', 'sp'), may hold values from -0.125 to 0.125
- gate_proj: bfloat16 [2, 1024, 2048], P(None, 'tp', 'sp'), may hold values from -0.125 to 0.125
- conv_taps: float32 [2, 4, 1024], P(None, None, 'tp'), may hold values from -3 to 3
- recur_map: bfloat16 [2, 16, 64, 64], P(None, 'tp'), may hold values from -0.75 to 0.75
- input_map: bfloat16 [2, 16, 64, 64], P(None, 'tp'), may hold values from -0.75 to 0.75
- decay_param: float32 [2, 1024], P(None, 'tp'), may hold values from 3 to 16
- decay_offset: float32 [2, 1024, 4096], P(None, 'tp', 'sp'), may hold values from -3 to 0
- mix_proj: bfloat16 [2, 1024, 2048], P(None, 'sp', 'tp'), may hold values from -0.1875 to 0.1875
Outputs:
- mixed_out: bfloat16 [8192, 2048], P(('grp', 'sp'), 'tp'), parts along dimension 0
There are 2 independent parts, one for each index of `grp`. A program takes and returns all parts, laid end to end along the dimension named above; an argument that names none is the same for every part. Nothing has to cross between parts.
All inputs are finite; a program needn't handle non-finite values.
Results may differ from a plain program's by a relative error of at most 0.013.
Values may be sent and summed in bfloat16 or wider, within the bound.
A program may use at most 64 MiB of HBM per device.

v0:
```python
import functools

import jax
import jax.numpy as jnp
from jax import lax
from jax.experimental import pallas as pl
from jax.experimental.pallas import tpu as pltpu
from jax.sharding import PartitionSpec as P

LAYERS = 2
EPS = 1e-06
RATE_SCALE = 8.0
LANES = 128
F32 = jnp.float32
BF16 = jnp.bfloat16


def log1p_series(u):
    z = u / (2.0 + u)
    zz = z * z
    acc = jnp.full_like(zz, 1.0 / 17.0)
    for n in (15, 13, 11, 9, 7, 5, 3, 1):
        acc = acc * zz + 1.0 / n
    return 2.0 * z * acc


def softplus(v):
    return jnp.maximum(v, 0.0) + log1p_series(jnp.exp(-jnp.abs(v)))


def minus_expm1(y, ey):
    acc = jnp.full_like(y, 1.0 / 8.0)
    for n in (7, 6, 5, 4, 3, 2):
        acc = (acc * y + 1.0) * (1.0 / n)
    small = -(acc * y + 1.0) * y
    return jnp.where(y > -0.4, small, 1.0 - ey)


def sigmoid(v):
    return 1.0 / (1.0 + jnp.exp(-v))


def half_turn(v):
    return pltpu.roll(v, LANES // 2, 1)


def twice(row):
    return jnp.concatenate([row, row], axis=1)


def scan_rows(a, b):
    rows = a.shape[0]
    at = lax.broadcasted_iota(jnp.int32, a.shape, 0)
    d = 1
    while d < rows:
        if d < 8:
            kept = at >= d
            b = b + a * jnp.where(kept, pltpu.roll(b, d, 0), 0.0)
            a = a * jnp.where(kept, pltpu.roll(a, d, 0), 1.0)
        else:
            b = jnp.concatenate([b[:d], b[d:] + a[d:] * b[:-d]], axis=0)
            a = jnp.concatenate([a[:d], a[d:] * a[:-d]], axis=0)
        d *= 2
    return a, b


def kernel(
    sp_n,
    tp_n,
    tok_ref,
    gain_ref,
    value_ref,
    gate_ref,
    taps_ref,
    recur_ref,
    input_ref,
    param_ref,
    offset_ref,
    mix_ref,
    out_ref,
    xbuf,
    bbuf,
    wbuf,
    bd,
    gw,
    offp,
    vpad,
    halo_out,
    halo_in,
    carry,
    zs,
    zr,
    xs,
    xr,
    hs,
    hr,
    cs,
    cr,
):
    sp = lax.axis_index("sp")
    tp = lax.axis_index("tp")
    core = lax.rem(tp, 2)
    chip = tp // 2
    partner = tp + 1 - 2 * core
    chips = tp_n // 2
    rounds = sp_n // 4
    tok = tok_ref.shape[0]
    half = tok // 2
    ch = value_ref.shape[1]

    def on_sp(step):
        return lax.rem(sp + (step + sp_n), sp_n)

    def on_tp(step):
        return 2 * lax.rem(chip + (step + chips), chips) + core

    offsets = [chips // 2]
    for k in range(1, chips // 2 + 1):
        offsets += [o for o in (chips // 2 + k, chips // 2 - k) if 0 < o < chips]

    barrier = pltpu.get_barrier_semaphore()
    z_steps = (1, 2, -1, -2) if sp_n > 4 else (1, 2, -1)
    for step in z_steps:
        pl.semaphore_signal(barrier, inc=1, device_id={"sp": on_sp(step)})
    for off in offsets:
        pl.semaphore_signal(barrier, inc=1, device_id={"tp": on_tp(off)})
    pl.semaphore_signal(barrier, inc=1, device_id={"tp": partner})
    peers = len(z_steps) + len(offsets) + 1

    def cols(j):
        return pl.ds(pl.multiple_of(j * LANES, LANES), LANES)

    def w_slot(layer):
        return lambda j: wbuf.at[layer, :, cols(j)]

    def m_slot(layer):
        return lambda j: bd.at[layer, pl.ds(pl.multiple_of(j * LANES, LANES), ch), pl.ds(0, LANES)]

    sends = []

    def put(src, dst, send, recv, **where):
        copy = pltpu.make_async_remote_copy(
            src_ref=src,
            dst_ref=dst,
            send_sem=send,
            recv_sem=recv,
            device_id=where,
            device_id_type=pl.DeviceIdType.MESH,
        )
        copy.start()
        sends.append(copy)

    def arrived(slot, sem):
        pltpu.make_async_copy(slot, slot, sem).wait()

    def z_round(stream, slot, k):
        moves = [(1, 0, -2 * k), (2, 1, -2 * k), (-1, 2, 2 * k)]
        if k < rounds - 1:
            moves.append((-2, 3, 2 * k))
        if k > 0:
            for block in (on_sp(-2 * k), on_sp(2 * k)):
                arrived(slot(block), zr.at[stream, block])
        for step, lane, off in moves:
            block = on_sp(off)
            put(slot(block), slot(block), zs.at[stream, k, lane], zr.at[stream, block], sp=on_sp(step))

    def z_finish(stream, slot):
        for k in range(rounds):
            for off in (-2 * k - 1, 2 * k + 1):
                arrived(slot(on_sp(off)), zr.at[stream, on_sp(off)])
        far = on_sp(-2 * rounds)
        arrived(slot(far), zr.at[stream, far])

    def x_start(g, slot):
        own = slot(tp)
        for n, off in enumerate(offsets):
            put(own, own, xs.at[g, n], xr.at[g, tp], tp=on_tp(off))
        put(own, own, xs.at[g, len(offsets)], xr.at[g, tp], tp=partner)

    def x_pass(g, slot, which):
        for n in which:
            block = on_tp(-offsets[n])
            arrived(slot(block), xr.at[g, block])
            put(slot(block), slot(block), xs.at[g, len(offsets) + 1 + n], xr.at[g, block], tp=partner)

    def x_finish(g, slot):
        for k in range(chips):
            block = 2 * k + (1 - core)
            arrived(slot(block), xr.at[g, block])

    lo8 = lax.broadcasted_iota(jnp.int32, (8, LANES), 1) < LANES // 2
    lo1 = lax.broadcasted_iota(jnp.int32, (1, LANES), 1) < LANES // 2
    lo = lax.broadcasted_iota(jnp.int32, (half, LANES), 1) < LANES // 2

    def own_weights(layer):
        gain = gain_ref[pl.ds(layer, 1), cols(sp)]
        both = jnp.concatenate([value_ref[layer], gate_ref[layer]], axis=0)
        wbuf[layer, :, cols(sp)] = (both.astype(F32) * gain).astype(BF16)

    def own_mix(layer):
        bd[layer, pl.ds(pl.multiple_of(sp * LANES, LANES), ch), 0:LANES] = mix_ref[layer]

    x_slot = lambda layer: (lambda j: xbuf.at[layer, :, cols(j)])
    b_slot = lambda layer: (lambda j: bbuf.at[layer, :, cols(j)])

    own_weights(0)
    xbuf[0, :, cols(tp)] = tok_ref[...]
    own_mix(0)
    own_weights(1)
    own_mix(1)

    pl.semaphore_wait(barrier, peers)
    z_round(0, w_slot(0), 0)
    x_start(0, x_slot(0))

    rates = []
    for layer in range(LAYERS):
        z64 = jnp.zeros((ch, LANES // 2), BF16)
        r, i = recur_ref[layer, 0], input_ref[layer, 0]
        gw[layer] = jnp.concatenate(
            [
                jnp.concatenate([r, z64, i, z64], axis=1),
                jnp.concatenate([z64, r, z64, i], axis=1),
            ],
            axis=0,
        )
        stacked = jnp.concatenate([offset_ref[layer, :, 0:half], offset_ref[layer, :, half:]], axis=0)
        offp[layer] = stacked.T
        rates.append(twice(-RATE_SCALE * softplus(-param_ref[pl.ds(layer, 1), :])))
        for j in range(tp_n):
            bd[layer, j * LANES : j * LANES + ch, LANES:] = jnp.zeros((ch, LANES), BF16)
            bd[layer, j * LANES + ch : (j + 1) * LANES, 0:LANES] = jnp.zeros((LANES - ch, LANES), BF16)

    def project(layer):
        total = jnp.zeros((tok, LANES), F32)
        for j in range(tp_n):
            block = xbuf[layer, :, j * LANES : (j + 1) * LANES].astype(F32)
            total = total + block * block
        scale = lax.rsqrt(jnp.sum(total, axis=1, keepdims=True) / (tp_n * LANES) + EPS)
        product = lax.dot_general(
            xbuf[layer], wbuf[layer], (((1,), (1,)), ((), ())), preferred_element_type=F32
        )
        return product * scale

    def halo_copy(layer):
        return pltpu.make_async_remote_copy(
            src_ref=halo_out.at[layer],
            dst_ref=halo_in.at[layer],
            send_sem=hs.at[layer],
            recv_sem=hr.at[layer],
            device_id={"sp": on_sp(1)},
            device_id_type=pl.DeviceIdType.MESH,
        )

    def carry_copy(layer, k):
        return pltpu.make_async_remote_copy(
            src_ref=carry.at[layer, sp],
            dst_ref=carry.at[layer, sp],
            send_sem=cs.at[layer, k],
            recv_sem=cr.at[layer, sp],
            device_id={"sp": k},
            device_id_type=pl.DeviceIdType.MESH,
        )

    def recurrence(layer, beside_carry):
        rows = project(layer)
        halo_out[layer] = rows[tok - 8 :]

        @pl.when(sp < sp_n - 1)
        def _():
            halo_copy(layer).start()

        top, bottom = rows[:half], rows[half:]
        values = jnp.where(lo, top, half_turn(bottom))
        gates = jnp.where(lo, half_turn(top), bottom)
        gated = gates * sigmoid(gates)
        vpad[8:, :] = values
        within = half_turn(top[half - 8 :])

        @pl.when(sp > 0)
        def _():
            halo_copy(layer).wait_recv()

        @pl.when(sp == 0)
        def _():
            halo_in[layer] = jnp.zeros((8, LANES), F32)

        vpad[0:8, :] = jnp.where(lo8, halo_in[layer], within)
        smoothed = jnp.zeros((half, LANES), F32)
        taps_n = taps_ref.shape[1]
        for k in range(taps_n):
            tap = twice(taps_ref[layer, k : k + 1, :])
            first = 8 - (taps_n - 1) + k
            smoothed = smoothed + tap * vpad[first : first + half, :]
        maps = jnp.dot(smoothed.astype(BF16), gw[layer], preferred_element_type=F32)
        recur = sigmoid(maps[:, :LANES])
        inputs = sigmoid(maps[:, LANES:])
        log_decay = recur * rates[layer] + offp[layer]
        decay = jnp.exp(log_decay)
        driving = jnp.sqrt(minus_expm1(2.0 * log_decay, decay * decay)) * inputs * smoothed
        a, b = scan_rows(decay, driving)
        a_end, b_end = a[half - 1 :], b[half - 1 :]
        a_turn, b_turn = half_turn(a_end), half_turn(b_end)
        whole = jnp.where(lo1, a_end * a_turn, half_turn(a_turn * b_end + b_turn))
        carry[layer, sp] = whole

        def send(k, _):
            carry_copy(layer, k).start()
            return 0

        lax.fori_loop(sp + 1, sp_n, send, 0)
        beside_carry()
        a, b = a * gated, b * gated

        def fold(k, state):
            arrived(carry.at[layer, k], cr.at[layer, k])
            row = carry[layer, k]
            return half_turn(row) + row * state

        state = lax.fori_loop(0, sp, fold, jnp.zeros((1, LANES), F32))
        state = jnp.where(lo1, state, half_turn(b_end + a_end * state))
        bbuf[layer, :, cols(tp)] = (b + a * state).astype(BF16)

    def mixed(layer):
        for j in range(tp_n):
            bd[layer, j * LANES + ch : (j + 1) * LANES, LANES:] = bd[layer, j * LANES : j * LANES + ch, 0:LANES]
        out = jnp.dot(bbuf[layer], bd[layer], preferred_element_type=F32)
        own = xbuf[layer, :, cols(tp)].astype(F32)
        both = jnp.concatenate([out[:, :LANES], out[:, LANES:]], axis=0)
        return (own + both).astype(BF16)

    def thirds(parts):
        n = len(offsets)
        return [range(n * p // parts, n * (p + 1) // parts) for p in range(parts)]

    pieces = thirds(rounds)
    for k in range(rounds):
        if k > 0:
            z_round(0, w_slot(0), k)
        if k == rounds - 1:
            z_round(1, m_slot(0), 0)
        x_pass(0, x_slot(0), pieces[k])
    x_finish(0, x_slot(0))
    z_finish(0, w_slot(0))

    def more(stream, slot, first, last):
        for k in range(first, min(last, rounds)):
            z_round(stream, slot, k)

    recurrence(0, lambda: more(1, m_slot(0), 1, 2))
    x_start(1, b_slot(0))
    more(1, m_slot(0), 2, 3)
    more(2, w_slot(1), 0, 1)
    a, b = thirds(2)
    x_pass(1, b_slot(0), a)
    more(1, m_slot(0), 3, rounds)
    more(2, w_slot(1), 1, 2)
    x_pass(1, b_slot(0), b)
    x_finish(1, b_slot(0))
    z_finish(1, m_slot(0))
    xbuf[1, :, cols(tp)] = mixed(0)
    x_start(2, x_slot(1))
    more(2, w_slot(1), 2, 3)
    more(3, m_slot(1), 0, 1)
    x_pass(2, x_slot(1), a)
    more(2, w_slot(1), 3, rounds)
    more(3, m_slot(1), 1, 2)
    x_pass(2, x_slot(1), b)
    x_finish(2, x_slot(1))
    z_finish(2, w_slot(1))
    recurrence(1, lambda: more(3, m_slot(1), 2, 3))
    x_start(3, b_slot(1))
    more(3, m_slot(1), 3, rounds)
    x_pass(3, b_slot(1), range(len(offsets)))
    x_finish(3, b_slot(1))
    z_finish(3, m_slot(1))
    out_ref[...] = mixed(1)

    for copy in sends:
        copy.wait_send()
    for layer in range(LAYERS):

        @pl.when(sp < sp_n - 1)
        def _():
            halo_copy(layer).wait_send()

        def sent(k, _):
            carry_copy(layer, k).wait_send()
            return 0

        lax.fori_loop(sp + 1, sp_n, sent, 0)


def solution(mesh):
    sp_n, tp_n = mesh.shape["sp"], mesh.shape["tp"]

    def local(*arrays):
        tok, wide = arrays[0].shape
        ch = arrays[2].shape[1]
        half = tok // 2
        full = tp_n * wide
        vmem = pl.BlockSpec(memory_space=pltpu.VMEM)
        dma = pltpu.SemaphoreType.DMA
        sent = 2 * (tp_n // 2)
        return pl.pallas_call(
            functools.partial(kernel, sp_n, tp_n),
            out_shape=jax.ShapeDtypeStruct((tok, wide), BF16),
            in_specs=[vmem] * len(arrays),
            out_specs=vmem,
            scratch_shapes=[
                pltpu.VMEM((LAYERS, tok, full), BF16),
                pltpu.VMEM((LAYERS, half, tp_n * LANES), BF16),
                pltpu.VMEM((LAYERS, 2 * ch, full), BF16),
                pltpu.VMEM((LAYERS, tp_n * LANES, 2 * LANES), BF16),
                pltpu.VMEM((LAYERS, 2 * ch, 2 * LANES), BF16),
                pltpu.VMEM((LAYERS, half, LANES), F32),
                pltpu.VMEM((half + 8, LANES), F32),
                pltpu.VMEM((LAYERS, 8, LANES), F32),
                pltpu.VMEM((LAYERS, 8, LANES), F32),
                pltpu.VMEM((LAYERS, sp_n, 1, LANES), F32),
                dma((2 * LAYERS, sp_n // 4, 4)),
                dma((2 * LAYERS, sp_n)),
                dma((2 * LAYERS, sent)),
                dma((2 * LAYERS, tp_n)),
                dma((LAYERS,)),
                dma((LAYERS,)),
                dma((LAYERS, sp_n)),
                dma((LAYERS, sp_n)),
            ],
            compiler_params=pltpu.CompilerParams(collective_id=0, has_side_effects=True),
        )(*arrays)

    in_specs = (
        P(("grp", "sp"), "tp"),
        P(),
        P(None, "tp", "sp"),
        P(None, "tp", "sp"),
        P(None, None, "tp"),
        P(None, "tp", None, None),
        P(None, "tp", None, None),
        P(None, "tp"),
        P(None, "tp", "sp"),
        P(None, "sp", "tp"),
    )
    out_specs = P(("grp", "sp"), "tp")
    return jax.shard_map(local, mesh=mesh, in_specs=in_specs, out_specs=out_specs, check_vma=False)
```

profile of v0, /device:TPU:80, one launch (start us, length us, event | category | flops | bytes accessed | tf_op | source)
XLA Modules:
  0.0 125.6 jit_solution(16248080311580834445)
XLA Ops:
  0.0 124.1 %shard_map.100 = bf16[256,128]{1,0:T(8,128)(2,1)} custom-call(bf16[256,128]{1,0:T(8,128)(2,1)} %tok_ref.1, f32[2,2048]{1,0:T(2,128)} %gain_ref.1, bf16[2,64,128]{2,1,0:T(8,128)(2,1)} %value_ref.1, bf16[2,64,128]{2,1,0:T(8,128)(2,1)} %gate_ref.1, f32[2,4,64]{2,1,0:T(4,128)} %taps_ref.1, bf16[2,1,64,64]{3,2,1,0:T(8,128)(2,1)} %recur_ref.1, ...), custom_call_target="tpu_custom_call" | custom-call | tf_op jit(solution)/shard_map/pallas_call | solution.py:405
  124.1 1.5 %copy.12 = bf16[256,128]{1,0:T(8,128)(2,1)} copy(bf16[256,128]{1,0:T(8,128)(2,1)} %shard_map.100) | data formatting | bytes 131072
where the time goes:
time: 126 us
  Pallas kernels  124 us (98%)
  local copies, waits for them, and re-layouts  1.47 us (1%)
    pallas_call x1, Pallas kernels, local(): pl.pallas_call(functools.partial(kernel, sp_n, tp_n), out_shape=jax.Shape...  124 us

commit v1 on v0

v1 whole, which is shorter than its diff:
```python
import functools

import jax
import jax.numpy as jnp
from jax import lax
from jax.experimental import pallas as pl
from jax.experimental.pallas import tpu as pltpu
from jax.sharding import PartitionSpec as P

LAYERS = 2
EPS = 1e-06
RATE_SCALE = 8.0
LANES = 128
F32 = jnp.float32
BF16 = jnp.bfloat16


def log1p_series(u):
    z = u / (2.0 + u)
    zz = z * z
    acc = jnp.full_like(zz, 1.0 / 17.0)
    for n in (15, 13, 11, 9, 7, 5, 3, 1):
        acc = acc * zz + 1.0 / n
    return 2.0 * z * acc


def softplus(v):
    return jnp.maximum(v, 0.0) + log1p_series(jnp.exp(-jnp.abs(v)))


def minus_expm1(y, ey):
    acc = jnp.full_like(y, 1.0 / 8.0)
    for n in (7, 6, 5, 4, 3, 2):
        acc = (acc * y + 1.0) * (1.0 / n)
    small = -(acc * y + 1.0) * y
    return jnp.where(y > -0.4, small, 1.0 - ey)


def sigmoid(v):
    return 1.0 / (1.0 + jnp.exp(-v))


def half_turn(v):
    return pltpu.roll(v, LANES // 2, 1)


def twice(row):
    return jnp.concatenate([row, row], axis=1)


def scan_rows(a, b):
    rows = a.shape[0]
    at = lax.broadcasted_iota(jnp.int32, a.shape, 0)
    d = 1
    while d < rows:
        if d < 8:
            kept = at >= d
            b = b + a * jnp.where(kept, pltpu.roll(b, d, 0), 0.0)
            a = a * jnp.where(kept, pltpu.roll(a, d, 0), 1.0)
        else:
            b = jnp.concatenate([b[:d], b[d:] + a[d:] * b[:-d]], axis=0)
            a = jnp.concatenate([a[:d], a[d:] * a[:-d]], axis=0)
        d *= 2
    return a, b


def kernel(sp_n, tp_n, *refs):
    (tok_hbm, gain_hbm, value_hbm, gate_hbm, taps_hbm, recur_hbm, input_hbm, param_hbm, offset_hbm, mix_hbm) = refs[:10]
    out_ref = refs[10]
    (gain_ref, value_ref, gate_ref, taps_ref, recur_ref, input_ref, param_ref, offset_ref, mix_ref) = refs[11:20]
    (xbuf, bbuf, wbuf, bd, gw, offp, vpad, squares, halo_out, halo_in, carry) = refs[20:31]
    (ls, zs, zr, xs, xr, hs, hr, cs, cr) = refs[31:]
    sp = lax.axis_index("sp")
    tp = lax.axis_index("tp")
    core = lax.rem(tp, 2)
    chip = tp // 2
    partner = tp + 1 - 2 * core
    chips = tp_n // 2
    stride = sp_n // 4
    hop = max(chips // 4, 1)
    tok = xbuf.shape[1]
    half = tok // 2
    ch = value_ref.shape[1]

    def on_sp(step):
        return lax.rem(sp + (step + sp_n), sp_n)

    def on_tp(step):
        return 2 * lax.rem(chip + (step + chips), chips) + core

    offsets = [chips // 2]
    for k in range(1, chips // 2 + 1):
        offsets += [o for o in (chips // 2 + k, chips // 2 - k) if 0 < o < chips]

    barrier = pltpu.get_barrier_semaphore()
    z_steps = [sign * step for step in range(stride, 0, -1) for sign in (1, -1)]
    for step in z_steps:
        pl.semaphore_signal(barrier, inc=1, device_id={"sp": on_sp(step)})
    for off in offsets:
        pl.semaphore_signal(barrier, inc=1, device_id={"tp": on_tp(off)})
    pl.semaphore_signal(barrier, inc=1, device_id={"tp": partner})
    peers = len(z_steps) + len(offsets) + 1

    def cols(j):
        return pl.ds(pl.multiple_of(j * LANES, LANES), LANES)

    local_copies = [
        pltpu.make_async_copy(src, dst, ls.at[n])
        for n, (src, dst) in enumerate(
            [
                (tok_hbm, xbuf.at[0, :, cols(tp)]),
                (gain_hbm, gain_ref),
                (value_hbm, value_ref),
                (gate_hbm, gate_ref),
                (mix_hbm, mix_ref),
                (taps_hbm, taps_ref),
                (recur_hbm, recur_ref),
                (input_hbm, input_ref),
                (param_hbm, param_ref),
                (offset_hbm, offset_ref),
            ]
        )
    ]
    for copy in local_copies:
        copy.start()

    def put(src, dst, send, recv, **where):
        pltpu.make_async_remote_copy(
            src_ref=src,
            dst_ref=dst,
            send_sem=send,
            recv_sem=recv,
            device_id=where,
            device_id_type=pl.DeviceIdType.MESH,
        ).start()

    def arrived(slot, sem):
        pltpu.make_async_copy(slot, slot, sem).wait()

    class Weights:
        def __init__(self, n, slot, many):
            self.n, self.slot, self.many = n, slot, many

        def send(self, block, step, relayed):
            n, slot = self.n, self.slot(block)
            lane = (0 if relayed > 0 else 1) if relayed else 2
            put(slot, slot, zs.at[n], zr.at[n, lane], sp=on_sp(step))

        def first(self):
            for step in z_steps:
                self.send(sp, step, step if abs(step) == stride else 0)

        def second(self):
            for sign, lane in ((1, 0), (-1, 1)):
                block = on_sp(-sign * stride)
                arrived(self.slot(block), zr.at[self.n, lane])
                for step in range(stride if sign > 0 else stride - 1, 0, -1):
                    self.send(block, sign * step, 0)

        def finish(self):
            arrived(self.many(sp_n - 3), zr.at[self.n, 2])

        def sent(self):
            arrived(self.many(sp_n - 1), zs.at[self.n])

    def w_rows(n, layer, first, count):
        return Weights(
            n,
            lambda j: wbuf.at[layer, first : first + count, cols(j)],
            lambda k: wbuf.at[layer, first : first + count, 0 : k * LANES],
        )

    def m_rows(n, layer):
        return Weights(
            n,
            lambda j: bd.at[layer, pl.ds(pl.multiple_of(j * LANES, LANES), ch), 0:LANES],
            lambda k: bd.at[layer, 0 : k * ch, 0:LANES],
        )

    w_value, w_gate, w_next = w_rows(0, 0, 0, ch), w_rows(1, 0, ch, ch), w_rows(2, 1, 0, 2 * ch)
    mixes = (m_rows(3, 0), m_rows(4, 1))

    class Tokens:
        def __init__(self, n, layer):
            self.n, self.layer = n, layer

        def slot(self, j, rows=None):
            return xbuf.at[self.layer, slice(0, tok) if rows is None else pl.ds(*rows), cols(j)]

        def put(self, lane, block, rows=None, **where):
            slot = self.slot(block, rows)
            put(slot, slot, xs.at[self.n], xr.at[self.n, lane], **where)

        def hand(self, block, lane):
            self.put(lane, block, tp=partner)

        def got(self, lane, block, rows=None):
            arrived(self.slot(block, rows), xr.at[self.n, lane])

        def first(self):
            for step in range(hop, 0, -1):
                self.put(2 + step, tp, tp=on_tp(step))
                if chips > 2:
                    self.put(2 + hop + step, tp, tp=on_tp(-step))
            self.hand(tp, 0)

        def second(self):
            if chips > 2:
                for sign in (1, -1):
                    block, at = on_tp(-sign * hop), 2 + (0 if sign > 0 else hop)
                    self.got(at + hop, block)
                    rows = (0 if sign > 0 else half, half)
                    self.put(3 + 2 * hop + (0 if sign > 0 else 1), block, rows, tp=on_tp(sign * hop))
                    for step in range(hop - 1, 0, -1):
                        self.put(4 + 2 * hop + (0 if sign > 0 else hop - 1) + step, block, tp=on_tp(sign * step))
                    self.hand(block, 0)
                    square(self.layer, block)
                for sign in (1, -1):
                    for step in range(1, hop):
                        block = on_tp(-sign * step)
                        self.got(2 + (0 if sign > 0 else hop) + step, block)
                        self.hand(block, 0)
                        square(self.layer, block)
            else:
                block = on_tp(1)
                self.got(2 + hop, block)
                self.hand(block, 0)
                square(self.layer, block)
            square(self.layer, tp)

        def third(self):
            if chips > 2:
                for sign in (1, -1):
                    for step in range(1, hop):
                        block = on_tp(-sign * (hop + step))
                        self.got(4 + 2 * hop + (0 if sign > 0 else hop - 1) + step, block)
                        self.hand(block, 1)
                        square(self.layer, block)
                block = on_tp(chips // 2)
                self.got(3 + 2 * hop, block, (0, half))
                self.got(4 + 2 * hop, block, (half, half))
                self.hand(block, 1)
                square(self.layer, block)

        def near(self):
            return 2 if chips == 2 else 1 + 2 * hop

        def finish(self):
            near = self.near()
            arrived(xbuf.at[self.layer, :, 0 : near * LANES], xr.at[self.n, 0])
            for step in range(-hop, hop + 1) if chips > 2 else (0, 1):
                square(self.layer, on_tp(step) + 1 - 2 * core)
            if chips > near:
                arrived(xbuf.at[self.layer, :, 0 : (chips - near) * LANES], xr.at[self.n, 1])
                for step in range(hop + 1, chips - hop):
                    square(self.layer, on_tp(step) + 1 - 2 * core)

        def sent(self):
            total = 2 * chips - 1
            arrived(xbuf.at[self.layer, :, 0 : total * LANES], xs.at[self.n])

    class Branches:
        def __init__(self, n, layer):
            self.n, self.layer = n, layer

        def put(self, lane, block, **where):
            slot = bbuf.at[self.layer, :, cols(block)]
            put(slot, slot, xs.at[self.n], xr.at[self.n, lane], **where)

        def first(self):
            for n, off in enumerate(offsets):
                self.put(1 + n, tp, tp=on_tp(off))
            self.put(0, tp, tp=partner)

        def second(self):
            for n, off in enumerate(offsets):
                block = on_tp(-off)
                arrived(bbuf.at[self.layer, :, cols(block)], xr.at[self.n, 1 + n])
                self.put(0, block, tp=partner)

        def finish(self):
            arrived(bbuf.at[self.layer, :, 0 : chips * LANES], xr.at[self.n, 0])

        def sent(self):
            arrived(bbuf.at[self.layer, :, 0 : (2 * chips - 1) * LANES], xs.at[self.n])

    lo8 = lax.broadcasted_iota(jnp.int32, (8, LANES), 1) < LANES // 2
    lo1 = lax.broadcasted_iota(jnp.int32, (1, LANES), 1) < LANES // 2

    def square(layer, block):
        wide = xbuf[layer, :, cols(block)].astype(F32)
        squares[...] += wide * wide

    def own_weights(layer):
        gain = gain_ref[pl.ds(layer, 1), cols(sp)]
        both = jnp.concatenate([value_ref[layer], gate_ref[layer]], axis=0)
        wbuf[layer, :, cols(sp)] = (both.astype(F32) * gain).astype(BF16)

    tokens = (Tokens(0, 0), Tokens(1, 1))
    branches = (Branches(2, 0), Branches(3, 1))

    for copy in local_copies[:4]:
        copy.wait()
    own_weights(0)
    pl.semaphore_wait(barrier, peers)
    w_value.first()
    tokens[0].first()
    w_gate.first()

    for copy in local_copies[4:]:
        copy.wait()
    own_weights(1)
    squares[...] = jnp.zeros((tok, LANES), F32)
    rates = []
    for layer in range(LAYERS):
        bd[layer, pl.ds(pl.multiple_of(sp * LANES, LANES), ch), 0:LANES] = mix_ref[layer]
        z64 = jnp.zeros((ch, LANES // 2), BF16)
        r, i = recur_ref[layer, 0], input_ref[layer, 0]
        gw[layer] = jnp.concatenate(
            [
                jnp.concatenate([r, z64, i, z64], axis=1),
                jnp.concatenate([z64, r, z64, i], axis=1),
            ],
            axis=0,
        )
        stacked = jnp.concatenate([offset_ref[layer, :, 0:half], offset_ref[layer, :, half:]], axis=0)
        offp[layer] = stacked.T
        rates.append(twice(-RATE_SCALE * softplus(-param_ref[pl.ds(layer, 1), :])))
        for j in range(tp_n):
            bd[layer, j * LANES : j * LANES + ch, LANES:] = jnp.zeros((ch, LANES), BF16)
            bd[layer, j * LANES + ch : (j + 1) * LANES, 0:LANES] = jnp.zeros((LANES - ch, LANES), BF16)

    def product(layer, rows, first):
        return lax.dot_general(
            xbuf[layer, rows, :],
            wbuf[layer, first : first + ch, :],
            (((1,), (1,)), ((), ())),
            preferred_element_type=F32,
        )

    def halo_copy(layer):
        return pltpu.make_async_remote_copy(
            src_ref=halo_out.at[layer],
            dst_ref=halo_in.at[layer],
            send_sem=hs.at[layer],
            recv_sem=hr.at[layer],
            device_id={"sp": on_sp(1)},
            device_id_type=pl.DeviceIdType.MESH,
        )

    def carry_copy(layer, k):
        return pltpu.make_async_remote_copy(
            src_ref=carry.at[layer, sp],
            dst_ref=carry.at[layer, sp],
            send_sem=cs.at[k],
            recv_sem=cr.at[layer, sp],
            device_id={"sp": k},
            device_id_type=pl.DeviceIdType.MESH,
        )

    def carries_sent(layer):
        def sent(k, _):
            carry_copy(layer, k).wait_send()
            return 0

        lax.fori_loop(sp + 1, sp_n, sent, 0)

    def elements(layer, first, count):
        smoothed = jnp.zeros((count, LANES), F32)
        taps_n = taps_ref.shape[1]
        for k in range(taps_n):
            tap = twice(taps_ref[layer, k : k + 1, :])
            at = 8 + first - (taps_n - 1) + k
            smoothed = smoothed + tap * vpad[at : at + count, :]
        maps = jnp.dot(smoothed.astype(BF16), gw[layer], preferred_element_type=F32)
        recur = sigmoid(maps[:, :LANES])
        inputs = sigmoid(maps[:, LANES:])
        log_decay = recur * rates[layer] + offp[layer, first : first + count, :]
        decay = jnp.exp(log_decay)
        driving = jnp.sqrt(minus_expm1(2.0 * log_decay, decay * decay)) * inputs * smoothed
        return scan_rows(decay, driving)

    def recurrence(layer, before_gates, after_carry):
        scale = lax.rsqrt(jnp.sum(squares[...], axis=1, keepdims=True) / (tp_n * LANES) + EPS)
        bottom = product(layer, slice(half, tok), 0) * scale[half:]
        halo_out[layer] = jnp.concatenate([bottom[half - 8 :], jnp.zeros((8, LANES - ch), F32)], axis=1)

        @pl.when(sp < sp_n - 1)
        def _():
            halo_copy(layer).start()

        top = product(layer, slice(0, half), 0) * scale[:half]
        values = jnp.concatenate([top, bottom], axis=1)
        vpad[8:, :] = values
        within = half_turn(values[half - 8 :])
        a, b = elements(layer, 8, half - 8)

        @pl.when(sp > 0)
        def _():
            halo_copy(layer).wait_recv()

        @pl.when(sp == 0)
        def _():
            halo_in[layer] = jnp.zeros((8, LANES), F32)

        vpad[0:8, :] = jnp.where(lo8, halo_in[layer], within)
        a8, b8 = elements(layer, 0, 8)
        b = b + a * b8[7:]
        a = a * a8[7:]
        a = jnp.concatenate([a8, a], axis=0)
        b = jnp.concatenate([b8, b], axis=0)
        a_end, b_end = a[half - 1 :], b[half - 1 :]
        a_turn, b_turn = half_turn(a_end), half_turn(b_end)
        whole = jnp.where(lo1, a_end * a_turn, half_turn(a_turn * b_end + b_turn))
        carry[layer, sp] = whole

        def send(k, _):
            carry_copy(layer, k).start()
            return 0

        lax.fori_loop(sp + 1, sp_n, send, 0)
        before_gates()
        gates = jnp.concatenate(
            [product(layer, slice(0, half), ch) * scale[:half], product(layer, slice(half, tok), ch) * scale[half:]],
            axis=1,
        )
        gated = gates * sigmoid(gates)
        a, b = a * gated, b * gated
        after_carry()

        def fold(k, state):
            arrived(carry.at[layer, k], cr.at[layer, k])
            row = carry[layer, k]
            return half_turn(row) + row * state

        state = lax.fori_loop(0, sp, fold, jnp.zeros((1, LANES), F32))
        state = jnp.where(lo1, state, half_turn(b_end + a_end * state))
        bbuf[layer, :, cols(tp)] = (b + a * state).astype(BF16)

    def second_place(layer):
        for j in range(tp_n):
            bd[layer, j * LANES + ch : (j + 1) * LANES, LANES:] = bd[layer, j * LANES : j * LANES + ch, 0:LANES]

    def mixed(layer):
        out = jnp.dot(bbuf[layer], bd[layer], preferred_element_type=F32)
        own = xbuf[layer, :, cols(tp)].astype(F32)
        both = jnp.concatenate([out[:, :LANES], out[:, LANES:]], axis=0)
        return (own + both).astype(BF16)

    tokens[0].second()
    w_value.second()
    w_gate.second()
    tokens[0].third()
    tokens[0].finish()
    w_value.finish()

    def gates_here():
        mixes[0].first()
        w_gate.finish()

    recurrence(0, gates_here, lambda: None)
    branches[0].first()
    mixes[0].second()
    w_next.first()
    squares[...] = jnp.zeros((tok, LANES), F32)
    branches[0].second()
    mixes[0].finish()
    second_place(0)
    branches[0].finish()
    xbuf[1, :, cols(tp)] = mixed(0)
    tokens[1].first()
    w_next.second()
    mixes[1].first()
    tokens[1].second()
    tokens[1].third()
    tokens[1].finish()
    w_next.finish()
    carries_sent(0)
    recurrence(1, lambda: None, mixes[1].second)
    branches[1].first()
    mixes[1].finish()
    second_place(1)
    branches[1].second()
    branches[1].finish()
    out_ref[...] = mixed(1)

    for weights in (w_value, w_gate, w_next, *mixes):
        weights.sent()
    for gather in (*tokens, *branches):
        gather.sent()
    carries_sent(1)
    for layer in range(LAYERS):

        @pl.when(sp < sp_n - 1)
        def _():
            halo_copy(layer).wait_send()


def solution(mesh):
    sp_n, tp_n = mesh.shape["sp"], mesh.shape["tp"]

    def local(*arrays):
        tok, wide = arrays[0].shape
        ch = arrays[2].shape[1]
        half = tok // 2
        full = tp_n * wide
        chips = tp_n // 2
        dma = pltpu.SemaphoreType.DMA
        return pl.pallas_call(
            functools.partial(kernel, sp_n, tp_n),
            out_shape=jax.ShapeDtypeStruct((tok, wide), BF16),
            in_specs=[pl.BlockSpec(memory_space=pl.ANY)] * len(arrays),
            out_specs=pl.BlockSpec(memory_space=pltpu.VMEM),
            scratch_shapes=[
                *(pltpu.VMEM(a.shape, a.dtype) for a in (*arrays[1:4], *arrays[4:])),
                pltpu.VMEM((LAYERS, tok, full), BF16),
                pltpu.VMEM((LAYERS, half, tp_n * LANES), BF16),
                pltpu.VMEM((LAYERS, 2 * ch, full), BF16),
                pltpu.VMEM((LAYERS, tp_n * LANES, 2 * LANES), BF16),
                pltpu.VMEM((LAYERS, 2 * ch, 2 * LANES), BF16),
                pltpu.VMEM((LAYERS, half, LANES), F32),
                pltpu.VMEM((half + 8, LANES), F32),
                pltpu.VMEM((tok, LANES), F32),
                pltpu.VMEM((LAYERS, 8, LANES), F32),
                pltpu.VMEM((LAYERS, 8, LANES), F32),
                pltpu.VMEM((LAYERS, sp_n, 1, LANES), F32),
                dma((len(arrays),)),
                dma((5,)),
                dma((5, 3)),
                dma((2 * LAYERS,)),
                dma((2 * LAYERS, max(chips + 3, 10))),
                dma((LAYERS,)),
                dma((LAYERS,)),
                dma((sp_n,)),
                dma((LAYERS, sp_n)),
            ],
            compiler_params=pltpu.CompilerParams(collective_id=0, has_side_effects=True),
        )(*arrays)

    in_specs = (
        P(("grp", "sp"), "tp"),
        P(),
        P(None, "tp", "sp"),
        P(None, "tp", "sp"),
        P(None, None, "tp"),
        P(None, "tp", None, None),
        P(None, "tp", None, None),
        P(None, "tp"),
        P(None, "tp", "sp"),
        P(None, "sp", "tp"),
    )
    out_specs = P(("grp", "sp"), "tp")
    return jax.shard_map(local, mesh=mesh, in_specs=in_specs, out_specs=out_specs, check_vma=False)
```

time: 126 us -> 107 us (0.85)
  the two profiles are of different devices: /device:TPU:80 before, /device:TPU:65 now
where the time goes in v1:
time: 107 us
  Pallas kernels  105 us (98%)
  local copies, waits for them, and re-layouts  1.47 us (1%)
    pallas_call x1, Pallas kernels, local(): pl.pallas_call(functools.partial(kernel, sp_n, tp_n), out_shape=jax.Shape...  105 us

profile of v1, /device:TPU:65, one launch (start us, length us, event | category | flops | bytes accessed | tf_op | source)
XLA Modules:
  0.0 106.7 jit_solution(18270513593355354767)
XLA Ops:
  0.0 105.2 %shard_map.100 = bf16[256,128]{1,0:T(8,128)(2,1)} custom-call(bf16[256,128]{1,0:T(8,128)(2,1)} %refs_0_.1, f32[2,2048]{1,0:T(2,128)} %refs_1_.1, bf16[2,64,128]{2,1,0:T(8,128)(2,1)} %refs_2_.1, bf16[2,64,128]{2,1,0:T(8,128)(2,1)} %refs_3_.1, f32[2,4,64]{2,1,0:T(4,128)} %refs_4_.1, bf16[2,1,64,64]{3,2,1,0:T(8,128)(2,1)} %refs_5_.1, ...), custom_call_target="tpu_custom_call" | custom-call | tf_op jit(solution)/shard_map/pallas_call | solution.py:509
  105.2 1.5 %copy.12 = bf16[256,128]{1,0:T(8,128)(2,1)} copy(bf16[256,128]{1,0:T(8,128)(2,1)} %shard_map.100) | data formatting | bytes 131072
